TPU v7x, 256 devices: a whole 4x4x8 slice. The times are simulated.
256 devices in a mesh: fs: 32 (over z, y), tp: 8 (over x, core).
Axes of the slice: x: 4, y: 4, z: 8, core: 2. Of those that a mesh axis runs over, the one named last changes fastest.
Arguments:
- x_next: bfloat16 [6144, 2048], P(('fs', 'tp')), may hold values from -6 to 6
- x_prev: bfloat16 [6144, 2048], P(('fs', 'tp')), may hold values from -6 to 6
- grad_out: bfloat16 [6144, 2048], P(('fs', 'tp')), may hold values from -24 to 24
- gate_w: bfloat16 [2048, 2816], P('fs', 'tp'), may hold values from -0.125 to 0.125
- up_w: bfloat16 [2048, 2816], P('fs', 'tp'), may hold values from -0.125 to 0.125
- down_w: bfloat16 [2816, 2048], P('tp', 'fs'), may hold values from -0.109375 to 0.109375
- acc_gate: float32 [2048, 2816], P('fs', 'tp'), may hold values from -2.5 to 2.5
- acc_up: float32 [2048, 2816], P('fs', 'tp'), may hold values from -2.5 to 2.5
- acc_down: float32 [2816, 2048], P('tp', 'fs'), may hold values from -2.5 to 2.5
Outputs:
- out_next: bfloat16 [6144, 2048], P(('fs', 'tp'))
- saved_hidden: bfloat16 [6144, 2816], P('fs', 'tp')
- grad_input: bfloat16 [6144, 2048], P(('fs', 'tp'))
- new_gate: float32 [2048, 2816], P('fs', 'tp')
- new_up: float32 [2048, 2816], P('fs', 'tp')
- new_down: float32 [2816, 2048], P('tp', 'fs')
All inputs are finite; a program needn't handle non-finite values.
Results may differ from a plain program's by a relative error of at most 0.014.
Values may be sent and summed in bfloat16 or wider, within the bound.
A program may use at most 64 MiB of HBM per device.

v0:
```python
import math

import jax
import jax.numpy as jnp
from jax import lax
from jax.sharding import Mesh
from jax.sharding import PartitionSpec as P

FS = ("fs_0", "fs_1")
FS_TP = ("fs_0", "fs_1", "tp")


def turned_gather(arrays, axis, dims):
    turned = [jnp.moveaxis(a, dim, 0) for a, dim in zip(arrays, dims)]
    both = jnp.concatenate([t.reshape(len(t), -1) for t in turned], axis=1)
    filled, at, gathered = (lax.all_gather(both, axis, axis=0, tiled=True), 0, [])
    for t, dim in zip(turned, dims):
        piece = filled[:, at : at + t[0].size].reshape(-1, *t.shape[1:])
        gathered.append(jnp.moveaxis(piece, 0, dim))
        at += t[0].size
    return tuple(gathered)


def sent_to_all(array, axis):
    length = lax.axis_size(axis)
    return lax.all_to_all(
        jnp.broadcast_to(array[None], (length, *array.shape)), axis, 0, 0, tiled=True
    )


def joined_along(blocks, dim):
    dims = list(blocks.shape[1:])
    dims[dim] *= blocks.shape[0]
    return jnp.moveaxis(blocks, 0, dim).reshape(dims)


def gather_directly(array, axis, dim):
    blocks = sent_to_all(array, axis)
    return joined_along(blocks, dim)


def cut_along(array, dim, length):
    dims = array.shape
    blocks = array.reshape(*dims[:dim], length, dims[dim] // length, *dims[dim + 1 :])
    return jnp.moveaxis(blocks, dim, 0)


def summed_on_arrival(array, axis, dim):
    blocks = cut_along(array, dim, lax.axis_size(axis))
    arrived = lax.all_to_all(blocks, axis, split_axis=0, concat_axis=0, tiled=True)
    return arrived.astype(jnp.float32).sum(axis=0)


def side_by_side(arrays, axis, dim, along):
    widths = [a.shape[along] for a in arrays]
    both = jnp.concatenate(arrays, axis=along)
    filled = lax.all_gather(both, axis, axis=dim, tiled=True)
    return tuple(jnp.split(filled, [sum(widths[:k]) for k in range(1, len(widths))], axis=along))


def sum_at_owner(array, axis, dim):
    length = lax.axis_size(axis)
    blocks = lax.all_to_all(cut_along(array, dim, length), axis, 0, 0, tiled=True)
    return jnp.sum(blocks, axis=0)


def sum_by_axis(running, axes):
    for axis in axes:
        running = lax.psum_scatter(running, axis, scatter_dimension=0, tiled=True)
    return running


def contract_rows(left, right):
    return lax.dot_general(
        left, right, (((0,), (0,)), ((), ())), preferred_element_type=jnp.float32
    )


def contract_cols(left, right):
    return lax.dot_general(
        left, right, (((1,), (1,)), ((), ())), preferred_element_type=jnp.float32
    )


def local(x_next, x_prev, grad_out, gate_w, up_w, down_w, acc_gate, acc_up, acc_down):
    local_rows = x_prev.shape[0]
    total_rows = local_rows * lax.axis_size("tp") * lax.axis_size(FS)
    factor = 1.0 / math.sqrt(total_rows)
    kept = turned_gather((gate_w, up_w, down_w), FS, (0, 0, 1))
    gate_full, up_full, down_full = kept
    piece = gather_directly(x_next, "tp", 0)
    gate = jnp.dot(piece, gate_full, preferred_element_type=jnp.float32)
    upper = jnp.dot(piece, up_full, preferred_element_type=jnp.float32)
    hidden = (jax.nn.silu(gate) * upper).astype(jnp.bfloat16)
    summed = summed_on_arrival(
        jnp.dot(hidden, down_full, preferred_element_type=jnp.float32).astype(jnp.bfloat16), "tp", 0
    )
    out_next = summed.astype(jnp.bfloat16)
    backward_gate_full, backward_up_full, backward_down_full = kept
    rows_prev, cotangent = side_by_side((x_prev, grad_out), "tp", 0, 1)
    gate_prev = jnp.dot(rows_prev, backward_gate_full, preferred_element_type=jnp.float32)
    up_prev = jnp.dot(rows_prev, backward_up_full, preferred_element_type=jnp.float32)
    grad_hidden = contract_cols(cotangent, backward_down_full)
    sigmoid_gate = jax.nn.sigmoid(gate_prev)
    silu_gate = gate_prev * sigmoid_gate
    grad_gate = (
        grad_hidden * up_prev * sigmoid_gate * (1.0 + gate_prev * (1.0 - sigmoid_gate))
    ).astype(jnp.bfloat16)
    grad_up = (grad_hidden * silu_gate).astype(jnp.bfloat16)
    hidden_prev = (silu_gate * up_prev).astype(jnp.bfloat16)
    columns = cotangent
    down_shard = sum_at_owner(contract_rows(columns, hidden_prev), FS, 0)
    new_down = acc_down + factor * down_shard.T
    stacked = jnp.concatenate((grad_gate, grad_up), axis=1)
    columns = rows_prev
    both_shard = sum_by_axis(contract_rows(columns, stacked), FS)
    width = grad_gate.shape[1]
    new_gate = acc_gate + factor * both_shard[:, :width]
    new_up = acc_up + factor * both_shard[:, width:]
    first = contract_cols(grad_gate, backward_gate_full)
    second = contract_cols(grad_up, backward_up_full)
    grad_input = summed_on_arrival((first + second).astype(jnp.bfloat16), "tp", 0).astype(
        jnp.bfloat16
    )
    grad_input, new_gate, new_up, new_down = (grad_input, new_gate, new_up, new_down)
    return (out_next, hidden, grad_input, new_gate, new_up, new_down)


def solution(mesh):
    split = Mesh(mesh.devices.reshape(8, 4, mesh.shape["tp"]), ("fs_0", "fs_1", "tp"))
    in_specs = (
        P(FS_TP, None),
        P(FS_TP, None),
        P(FS_TP, None),
        P(FS, "tp"),
        P(FS, "tp"),
        P("tp", FS),
        P(FS, "tp"),
        P(FS, "tp"),
        P("tp", FS),
    )
    out_specs = (P(FS_TP, None), P(FS, "tp"), P(FS_TP, None), P(FS, "tp"), P(FS, "tp"), P("tp", FS))
    return jax.shard_map(local, mesh=split, in_specs=in_specs, out_specs=out_specs, check_vma=False)
```

profile of v0, /device:TPU:1, one launch (start us, length us, event | category | flops | bytes accessed | tf_op | source)
XLA Modules:
  0.0 282.7 jit_solution(2041042809209403045)
XLA Ops:
  7.2 1.6 pad_maximum_fusion
  8.9 0.0 all-gather.3.cloned.1.call-start
  8.9 1.6 concatenate.9
  10.6 30.3 %all-gather.5.cloned.1.call-done = bf16[192,4096]{1,0:T(8,128)(2,1)} async-done(((bf16[24,4096]{1,0:T(8,128)(2,1)}), bf16[192,4096]{1,0:T(8,128)(2,1)}) %all-gather.5.cloned.1.call-update) | async-done | bytes 1572880 | tf_op jit(solution)/shard_map/all_gather | solution.py:57
  40.9 82.3 %all-gather.3.cloned.1.call-done = bf16[2048,1056]{1,0:T(8,128)(2,1)} async-done(((bf16[64,1056]{1,0:T(8,128)(2,1)}), bf16[2048,1056]{1,0:T(8,128)(2,1)}) %all-gather.3.cloned.1.call-update) | async-done | bytes 4325392 | tf_op jit(solution)/shard_map/all_gather | solution.py:16
  123.2 2.2 fusion.11
  125.4 2.4 fusion.5
  127.8 2.5 multiply_convert_fusion.1
  130.3 3.6 %fusion.30 = f32[2048,704]{0,1:T(8,128)} fusion(bf16[192,4096]{1,0:T(8,128)(2,1)S(1)} %copy-done.2, bf16[192,352]{1,0:T(8,128)(2,1)S(1)} %get-tuple-element.18, bf16[192,352]{1,0:T(8,128)(2,1)S(1)} %get-tuple-element.19), kind=kOutput, calls=%fused_computation.24 | convolution fusion | flops 554188800 | bytes 6848512 | tf_op jit(solution)/shard_map/dot_general | solution.py:74
  134.0 0.9 copy-done.5
  134.9 0.1 broadcast_in_dim.2
  134.9 20.6 %all_to_all.20 = bf16[8,24,2048]{2,1,0:T(8,128)(2,1)S(1)} all-to-all(bf16[8,24,2048]{2,1,0:T(8,128)(2,1)S(1)} %broadcast_in_dim.2), channel_id=1, replica_groups=mesh['fs_0'=8,'fs_1'=4,'tp'=8] {'tp'}, dimensions={0} | all-to-all | bytes 1572864 | tf_op jit(solution)/shard_map/all_to_all | solution.py:26
  155.6 2.0 fusion.15
  157.5 2.4 fusion.24
  160.0 3.4 %convolution_convert_fusion = bf16[192,2048]{1,0:T(8,128)(2,1)} fusion(bf16[192,352]{1,0:T(8,128)(2,1)S(1)} %fusion.24, bf16[2048,1056]{1,0:T(8,128)(2,1)} %all-gather.3.cloned.1.call-done), kind=kOutput, calls=%fused_computation.2 | convolution fusion | flops 277217280 | bytes 2494464 | tf_op jit(solution)/shard_map/dot_general | solution.py:96
  163.4 4.4 %all-to-all-start.1 = ((bf16[8,24,2048]{2,1,0:T(8,128)(2,1)}), bf16[8,24,2048]{2,1,0:T(8,128)(2,1)S(1)}, u32[]{:S(2)}, u32[]{:S(2)}) async-start(bf16[8,24,2048]{2,1,0:T(8,128)(2,1)} %bitcast.4), calls=%async_computation.1 | async-start | bytes 1572864 | tf_op jit(solution)/shard_map/all_to_all | solution.py:50
  167.8 2.2 fusion.9
  169.9 3.4 %fusion = bf16[192,2048]{1,0:T(8,128)(2,1)} fusion(f32[192,2048]{1,0:T(8,128)S(1)} %fusion.9, bf16[192,352]{1,0:T(8,128)(2,1)S(1)} %get-tuple-element.18, bf16[2048,1056]{1,0:T(8,128)(2,1)} %all-gather.3.cloned.1.call-done), kind=kOutput, calls=%fused_computation.1 | convolution fusion | flops 277610496 | bytes 4067328 | tf_op jit(solution)/shard_map/dot_general | solution.py:80
  173.3 6.6 %all-to-all-done.1 = bf16[8,24,2048]{2,1,0:T(8,128)(2,1)S(1)} async-done(((bf16[8,24,2048]{2,1,0:T(8,128)(2,1)}), bf16[8,24,2048]{2,1,0:T(8,128)(2,1)S(1)}, u32[]{:S(2)}, u32[]{:S(2)}) %all-to-all-start.1) | async-done | bytes 786464 | tf_op jit(solution)/shard_map/all_to_all | solution.py:50
  180.0 4.4 %all-to-all-start.2 = ((bf16[8,24,2048]{2,1,0:T(8,128)(2,1)}), bf16[8,24,2048]{2,1,0:T(8,128)(2,1)S(1)}, u32[]{:S(2)}, u32[]{:S(2)}) async-start(bf16[8,24,2048]{2,1,0:T(8,128)(2,1)} %bitcast.5), calls=%async_computation.2 | async-start | bytes 1572864 | tf_op jit(solution)/shard_map/all_to_all | solution.py:50
  184.4 3.4 %fusion.27 = f32[2048,352]{1,0:T(8,128)} fusion(bf16[192,4096]{1,0:T(8,128)(2,1)S(1)} %copy-done.2, f32[192,352]{1,0:T(8,128)} %copy-done.3, f32[192,352]{1,0:T(8,128)S(1)} %fusion.11), kind=kOutput, calls=%fused_computation.21 | convolution fusion | flops 277229568 | bytes 4235264 | tf_op jit(solution)/shard_map/dot_general | solution.py:74
  187.8 8.7 %all-to-all-done.2 = bf16[8,24,2048]{2,1,0:T(8,128)(2,1)S(1)} async-done(((bf16[8,24,2048]{2,1,0:T(8,128)(2,1)}), bf16[8,24,2048]{2,1,0:T(8,128)(2,1)S(1)}, u32[]{:S(2)}, u32[]{:S(2)}) %all-to-all-start.2) | async-done | bytes 786464 | tf_op jit(solution)/shard_map/all_to_all | solution.py:50
  196.6 0.9 copy-done.1
  197.5 5.5 %all-to-all-start.3 = ((f32[32,64,352]{2,1,0:T(8,128)}), f32[32,64,352]{2,1,0:T(8,128)S(1)}, u32[]{:S(2)}, u32[]{:S(2)}) async-start(f32[32,64,352]{2,1,0:T(8,128)} %bitcast.6), calls=%async_computation.4 | async-start | bytes 6291456 | tf_op jit(solution)/shard_map/all_to_all | solution.py:63
  203.0 2.1 reduce-scatter.5.cloned.1.call-done
  205.1 2.3 copy.32
  207.4 1.9 reduce_sum.33
  209.3 1.9 reduce_sum.34
  211.2 62.3 %all-to-all-done.3 = f32[32,64,352]{2,1,0:T(8,128)S(1)} async-done(((f32[32,64,352]{2,1,0:T(8,128)}), f32[32,64,352]{2,1,0:T(8,128)S(1)}, u32[]{:S(2)}, u32[]{:S(2)}) %all-to-all-start.3) | async-done | bytes 2883616 | tf_op jit(solution)/shard_map/all_to_all | solution.py:63
  273.6 0.2 reduce_sum.35
  273.8 0.7 bitcast_add_fusion
  274.4 1.7 fusion.38
  (24 shorter events, 0.2 us)
Async XLA Ops:
  7.2 33.8 %all-gather.5.cloned.1.call-start = ((), (), s32[]{:S(2)}) async-start(), calls=%async_computation.7 | async-start | bytes 1769472 | tf_op jit(solution)/shard_map/all_gather | solution.py:57
  8.9 114.3 %all-gather.3.cloned.1.call-start = ((), (), s32[]{:S(2)}) async-start(), calls=%async_computation.6 | async-start | bytes 4866048 | tf_op jit(solution)/shard_map/all_gather | solution.py:16
  10.6 194.5 %reduce-scatter.5.cloned.1.call-start = ((), (), s32[]{:S(2)}) async-start(), calls=%async_computation.8 | async-start | bytes 6488064 | tf_op jit(solution)/shard_map/reduce_scatter | solution.py:69
  40.9 84.5 %copy-start.2 = (bf16[192,4096]{1,0:T(8,128)(2,1)S(1)}, bf16[192,4096]{1,0:T(8,128)(2,1)}, u32[]{:S(2)}) copy-start(bf16[192,4096]{1,0:T(8,128)(2,1)} %all-gather.5.cloned.1.call-done) | copy-start | bytes 4718596
  127.8 2.5 copy-start.3
  134.0 0.9 copy-start.5
  160.0 3.4 %copy-start.4 = (bf16[192,352]{1,0:T(8,128)(2,1)}, bf16[192,352]{1,0:T(8,128)(2,1)S(1)}, u32[]{:S(2)}) copy-start(bf16[192,352]{1,0:T(8,128)(2,1)S(1)} %fusion.24) | copy-start | bytes 405508
  163.4 16.6 %all-to-all-start.1 = ((bf16[8,24,2048]{2,1,0:T(8,128)(2,1)}), bf16[8,24,2048]{2,1,0:T(8,128)(2,1)S(1)}, u32[]{:S(2)}, u32[]{:S(2)}) async-start(bf16[8,24,2048]{2,1,0:T(8,128)(2,1)} %bitcast.4), calls=%async_computation.1 | async-start | bytes 1572864 | tf_op jit(solution)/shard_map/all_to_all | solution.py:50
  180.0 7.9 %copy-start = (bf16[8,24,2048]{2,1,0:T(8,128)(2,1)}, bf16[8,24,2048]{2,1,0:T(8,128)(2,1)S(1)}, u32[]{:S(2)}) copy-start(bf16[8,24,2048]{2,1,0:T(8,128)(2,1)S(1)} %all-to-all-done.1) | copy-start | bytes 2359300
  180.0 16.6 %all-to-all-start.2 = ((bf16[8,24,2048]{2,1,0:T(8,128)(2,1)}), bf16[8,24,2048]{2,1,0:T(8,128)(2,1)S(1)}, u32[]{:S(2)}, u32[]{:S(2)}) async-start(bf16[8,24,2048]{2,1,0:T(8,128)(2,1)} %bitcast.5), calls=%async_computation.2 | async-start | bytes 1572864 | tf_op jit(solution)/shard_map/all_to_all | solution.py:50
  196.6 0.9 copy-start.1
  197.5 76.1 %all-to-all-start.3 = ((f32[32,64,352]{2,1,0:T(8,128)}), f32[32,64,352]{2,1,0:T(8,128)S(1)}, u32[]{:S(2)}, u32[]{:S(2)}) async-start(f32[32,64,352]{2,1,0:T(8,128)} %bitcast.6), calls=%async_computation.4 | async-start | bytes 6291456 | tf_op jit(solution)/shard_map/all_to_all | solution.py:63
  202.9 71.5 %reduce-scatter.7.cloned.1.call-start = ((), (), s32[]{:S(2)}) async-start(), calls=%async_computation.9 | async-start | bytes 983040 | tf_op jit(solution)/shard_map/reduce_scatter | solution.py:69
  211.2 62.5 %copy-start.8 = (f32[352,64]{0,1:T(8,128)S(1)}, f32[352,64]{0,1:T(8,128)}, u32[]{:S(2)}) copy-start(f32[352,64]{0,1:T(8,128)} %param.17) | copy-start | bytes 270340
  211.2 63.2 %copy-start.6 = (f32[64,352]{1,0:T(8,128)S(1)}, f32[64,352]{1,0:T(8,128)}, u32[]{:S(2)}) copy-start(f32[64,352]{1,0:T(8,128)} %param.16) | copy-start | bytes 270340
  211.2 63.2 %copy-start.7 = (f32[64,352]{1,0:T(8,128)S(1)}, f32[64,352]{1,0:T(8,128)}, u32[]{:S(2)}) copy-start(f32[64,352]{1,0:T(8,128)} %param.15) | copy-start | bytes 270340
Sparse Core Ops, SparseCore 0:
  9.8 31.0 all-gather.4
  44.1 79.0 all-gather.2
  134.1 70.9 reduce-scatter.4
  207.5 30.5 reduce-scatter.6
where the time goes:
time: 284 us; the launch traced here: 283 us
  waiting for transfers between devices  192 us (68%)
  matrix products  27.5 us (10%)
  blocking collectives  20.6 us (7%)
  starting transfers between devices  14.5 us (5%)
  between operations  13.9 us (5%)
  other arithmetic  7.99 us (3%)
  local copies, waits for them, and re-layouts  5.77 us (2%)
    all_gather x1, waiting for transfers between devices, turned_gather(): lax.all_gather(both, axis, axis=0, tiled=True)  82.3 us
    all_to_all x1, waiting for transfers between devices, sum_at_owner(): lax.all_to_all(cut_along(array, dim, length), axis, 0, 0, tiled=True)  62.3 us
    all_gather x1, waiting for transfers between devices, side_by_side(): filled = lax.all_gather(both, axis, axis=dim, tiled=True)  30.3 us
    all_to_all x1, blocking collectives, sent_to_all(): lax.all_to_all(jnp.broadcast_to(array[None], (length, *array.shape)), axi...  20.6 us
    all_to_all x2, waiting for transfers between devices, summed_on_arrival(): lax.all_to_all(blocks, axis, split_axis=0, concat_axis=0, tiled=True)  15.4 us
    all_to_all x2, starting transfers between devices, summed_on_arrival(): lax.all_to_all(blocks, axis, split_axis=0, concat_axis=0, tiled=True)  8.84 us
    dot_general x3, matrix products, contract_cols(): lax.dot_general(left, right, (((1,), (1,)), ((), ())), preferred_element_...  8.04 us
    dot_general x2, matrix products, contract_rows(): lax.dot_general(left, right, (((0,), (0,)), ((), ())), preferred_element_...  7.08 us
  transfers between devices with their start and end apart: 7, of which 6 were waited for; matrix products, arithmetic and copies ran while one was open for 9% of the time, Pallas kernels for 0%

commit v1 on v0

v1 whole, which is shorter than its diff:
```python
import functools
import heapq
import math

import jax
import jax.numpy as jnp
from jax import lax
from jax.experimental import pallas as pl
from jax.experimental.pallas import tpu as pltpu
from jax.sharding import Mesh
from jax.sharding import PartitionSpec as P

MESH = pl.DeviceIdType.MESH
F32, BF16 = jnp.float32, jnp.bfloat16
TOK = ("z", "y", "x", "c")
FS, TP = ("z", "y"), ("x", "c")
NZ, NY, NX, NC = 8, 4, 4, 2
NB = NX * NC
ROWS, HALF = 64, 32
UNITS = 352
SEG = 384
WIDE = 3 * SEG
ZB = NY * ROWS
TOKENS = 24
GROUP = NB * TOKENS
LATE = 5
LATENCY, ROW_US = 1.8, 1.0 / 20.2

EZ = (0, 1, -1, 2, -2, 3, -3, 4)
EY = (0, 1, -1, 2)
REDUCE = (
    (4, 2), (3, 2), (-3, 2), (-2, 2), (4, -1), (4, 1), (3, -1), (-1, 2), (2, 2), (-3, -1), (3, 1), (-3, 1), (-2, -1),
    (1, 2), (-2, 1), (4, 0), (2, -1), (2, 1), (0, 2), (-3, 0), (3, 0), (-1, 1), (-1, -1), (-2, 0), (1, -1), (2, 0),
    (1, 1), (0, -1), (0, 1), (-1, 0), (1, 0),
)


def rows_of(m):
    ez, ey = m
    if abs(ey) == 2:
        return (0, HALF // 2) if ey > 0 else (HALF // 2, HALF)
    if ey == 0 and abs(ez) == 4:
        return (0, HALF // 2) if ez > 0 else (HALF // 2, HALF)
    return 0, HALF


def sends_of(n):
    ez, ey = n
    if abs(ey) == 1:
        return [(ez, 2 * ey)]
    if ey:
        return []
    along_y = [(ez, 1), (ez, -1)]
    if abs(ez) in (1, 2):
        return along_y + [(ez + (2 if ez > 0 else -2), 0)]
    return along_y


def node_of(m):
    ez, ey = m
    return (abs(ez) if ez == -4 else ez, abs(ey) if ey == -2 else ey)


def parts_of(n):
    ez, ey = n
    if ey == 2:
        return [(ez, 2), (ez, -2)]
    return [(4, 0), (-4, 0)] if n == (4, 0) else [n]


def step_of(m):
    ez, ey = m
    if ey:
        return "y", 1 if ey > 0 else -1
    return "z", (1 if abs(ez) == 1 else 2) * (1 if ez > 0 else -1)


@functools.lru_cache
def gather_plan():
    free, heap, got, order, ends = {}, [], set(), [], {}

    def push(now, m):
        axis, step = step_of(m)
        lo, hi = rows_of(m)
        cost = (hi - lo) * ROW_US * abs(step) if abs(m[0]) > 2 or m[1] else HALF * ROW_US * abs(step)
        link = axis, step > 0
        free[link] = max(now, free.get(link, 0.0)) + cost
        ends[m] = free[link]
        heapq.heappush(heap, (free[link] + LATENCY + 0.7 * (abs(step) - 1), len(ends), m))

    def issue(now, n):
        order.append((n, now))
        for m in sends_of(n):
            if m == (3, 0):
                push(now, (2, 0))
                push(now, (-2, 0))
            push(now, m)

    push(0.0, (1, 0))
    push(0.0, (-1, 0))
    issue(0.5, (0, 0))
    while heap:
        t, _, m = heapq.heappop(heap)
        got.add(m)
        if all(q in got for q in parts_of(node_of(m))):
            issue(t, node_of(m))
    ids = {m: i for i, m in enumerate(ends)}
    return order, ids


def layer(
    xn_in, xp_in, go_in, gw_in, uw_in, dw_in,
    out_ref, hid_ref, gin_ref, wg_out,
    mine, ours, own, w, tok, xpt, got, accp, accn, gg, hp, hid, hidv, gb, gr, s, r, far_sum, home_in, home,
    part, ring, ringed, plane, crossed, outv,
    ag_s, ag_r, home_s, home_r, twin_s, twin_r, hop_s, hop_r, tk_s, tk_r,
    gift_s, gift_r, rs_s, rs_r, top_s, top_r, back_s, back_r, ring_s, ring_r, plane_s, plane_r,
    hid_s, hid_r, out_s, in_s,
):
    z, y, x, c = (lax.axis_index(a) for a in ("z", "y", "x", "c"))
    par = lax.rem(z, 2)
    zp = z + 1 - 2 * par
    j = x * NC + c
    me = z * NY + y
    keeps = c == par
    moves = c != par
    size = {"z": NZ, "y": NY, "x": NX}
    here = {"z": z, "y": y, "x": x}

    def at(axis, step):
        return lax.rem(here[axis] + (step + size[axis]), size[axis])

    barrier = pltpu.get_barrier_semaphore()
    friends = [{"z": at("z", d), "c": q} for d in (1, -1, 2, -2) for q in range(NC)]
    friends += [{"y": at("y", 1)}, {"y": at("y", -1)}, {"x": at("x", 1)}, {"x": at("x", -1)}, {"c": 1 - c}]
    for friend in friends:
        pl.semaphore_signal(barrier, inc=1, device_id=friend, device_id_type=MESH)

    loads = [(ref, ours.at[i]) for i, ref in enumerate((gw_in, uw_in, dw_in))]
    loads += [(ref, mine.at[i]) for i, ref in enumerate((xp_in, go_in, xn_in))]
    loads = [pltpu.make_async_copy(src, dst, in_s.at[i]) for i, (src, dst) in enumerate(loads)]
    for copy in loads:
        copy.start()

    own[...] = jnp.zeros((NC, HALF, WIDE), BF16)
    for copy in loads:
        copy.wait()
    for q in range(NC):
        for i in range(3):
            own[q, :, SEG * i:SEG * i + UNITS] = ours[i, HALF * q:HALF * q + HALF, :]

    @pl.when(keeps)
    def _():
        w[me] = own[...]
        for a in range(3):
            tok[NB * a + j] = mine[a]

    with jax.named_scope("barrier"):
        pl.semaphore_wait(barrier, len(friends))

    def remote(src, dst, ssem, rsem, device):
        pltpu.make_async_remote_copy(
            src_ref=src, dst_ref=dst, send_sem=ssem, recv_sem=rsem, device_id=device, device_id_type=MESH
        ).start()

    def expect(dst, sem):
        pltpu.make_async_copy(dst, dst, sem).wait()

    order, ids = gather_plan()

    def chunk_at(n):
        return at("z", -n[0]) * NY + at("y", -n[1])

    def own_sends(step):
        for sign in (1, -1):
            for q in range(NC):
                remote(
                    own.at[q], w.at[me, q], top_s, ag_r.at[ids[(sign * step, 0)]],
                    {"z": at("z", sign * step), "c": q},
                )

    @pl.when(keeps)
    def _():
        remote(own, w.at[me], home_s, home_r, {"c": 1 - c})

    @pl.when(moves)
    def _():
        own_sends(1)

    @pl.when(moves)
    def _():
        for a in range(3):
            remote(mine.at[a], tok.at[NB * a + j], hop_s, hop_r.at[a, c], {"c": 1 - c})

    def hop(a):
        block = tok.at[NB * a + j]

        @pl.when(moves)
        def _():
            remote(mine.at[a], block, hop_s, hop_r.at[a, c], {"z": zp, "c": 1 - c})

        @pl.when(keeps)
        def _():
            remote(mine.at[a], block, hop_s, hop_r.at[a, c], {"z": zp})

    hop(0)

    @pl.when(moves)
    def _():
        expect(w.at[me], home_r)

    def forward(n):
        ch = chunk_at(n)
        for m in sends_of(n):
            if m == (3, 0):

                @pl.when(keeps)
                def _():
                    own_sends(2)

                hop(1)

            lo, hi = rows_of(m)
            piece = w.at[ch, c, pl.ds(lo, hi - lo)]
            axis, step = step_of(m)
            remote(piece, piece, ag_s, ag_r.at[ids[m]], {axis: at(axis, step)})
        if n != (0, 0):
            remote(w.at[ch, c], w.at[ch, c], twin_s, twin_r.at[EZ.index(n[0])], {"c": 1 - c})

    def tok_pair(a):
        pair = tok.at[pl.ds(NB * a + x * NC, NC)]
        for i, sign in enumerate((1, -1)):
            remote(pair, pair, tk_s, tk_r.at[a, i], {"x": at("x", sign)})

    def tok_stay(a):
        @pl.when(keeps)
        def _():
            expect(tok.at[NB * a + x * NC + 1 - c], hop_r.at[a, 1 - c])
            tok_pair(a)

    def tok_hop(a):
        @pl.when(moves)
        def _():
            for q in range(NC):
                expect(tok.at[NB * a + x * NC + q], hop_r.at[a, q])
            tok_pair(a)

    def tok_near(a, who):
        @pl.when(who)
        def _():
            for i, sign in enumerate((1, -1)):
                first = NB * a + at("x", -sign) * NC
                expect(tok.at[pl.ds(first, NC)], tk_r.at[a, i])
                block = tok.at[first + i]
                remote(block, block, tk_s, tk_r.at[a, 2 + i], {"x": at("x", sign)})

    def tok_far(a):
        for i in range(2):
            expect(tok.at[NB * a + at("x", 2) * NC + i], tk_r.at[a, 2 + i])

    def cols(zb):
        return pl.ds(pl.multiple_of(zb * ZB, ZB), ZB)

    def weights(zb):
        return w[pl.ds(zb * NY, NY)].reshape(ZB, WIDE)

    eye_zb = (
        lax.broadcasted_iota(jnp.int32, (ZB, ZB), 0) == lax.broadcasted_iota(jnp.int32, (ZB, ZB), 1)
    ).astype(BF16)

    def turn(a, dst, zb):
        block = tok[NB * a:NB * a + NB, :, cols(zb)].reshape(GROUP, ZB)
        dst[zb] = lax.dot_general(
            eye_zb, block, (((1,), (1,)), ((), ())), preferred_element_type=F32
        ).astype(BF16)

    def project(a, acc, lanes, zb, first):
        block = tok[NB * a:NB * a + NB, :, cols(zb)].reshape(GROUP, ZB)
        value = jnp.dot(block, weights(zb)[:, lanes[0]:lanes[1]], preferred_element_type=F32)
        if first:
            acc[:, lanes[0]:lanes[1]] = value
        else:
            acc[:, lanes[0]:lanes[1]] += value

    def block_steps(e):
        return (e,) if e in (0, 4) else (e, -e)

    done = set()
    turns = [functools.partial(turn, a, dst, at("z", -ez)) for a, dst in ((0, xpt), (1, got)) for ez in EZ[NZ - LATE:]]

    def project_block(a, e):
        for ez in block_steps(e):
            if ez not in twins:
                count = NY - 1 if ez == 0 else NY
                expect(w.at[pl.ds(0, count), 1 - c], twin_r.at[EZ.index(ez)])
                twins.add(ez)
            project(a, accp, ((0, 2 * SEG), (2 * SEG, WIDE))[a], at("z", -ez), ez == 0)
        done.add((a, e))

    twins, ready = set(), set()

    def fill(i):
        for a in range(2):
            for e in range(5):
                if a in ready and (a, e) not in done and i > last_of[e]:
                    project_block(a, e)
                    break
        for _ in range(2):
            if turns and (1 if len(turns) <= LATE else 0) in ready:
                turns.pop(0)()

    last_of = {
        e: max(i for i, (n, _) in enumerate(order) if abs(n[0]) == e) for e in range(5)
    }

    def tok_last(a):
        tok_far(a)
        ready.add(a)

    timed = [
        (1.0, tok_stay, 0), (1.1, tok_stay, 1), (6.4, tok_near, 0, keeps), (6.6, tok_hop, 0), (9.0, tok_near, 1, keeps),
        (9.1, hop, 2), (10.9, tok_hop, 1), (11.0, tok_near, 0, moves), (15.0, tok_near, 1, moves), (15.1, tok_stay, 2),
        (15.2, tok_hop, 2), (16.0, tok_last, 0), (19.7, tok_last, 1), (22.5, tok_near, 2, c >= 0),
    ]
    for i, (n, t) in enumerate(order):
        while timed and timed[0][0] <= (t if i + 1 < len(order) else 99):
            when, work, *given = timed.pop(0)
            with jax.named_scope("t#%s%.1f" % (work.__name__, when)):
                work(*given)
        with jax.named_scope("ga#i=%d#z=%d#y=%d" % (i, *n)):
            if n != (0, 0):
                for m in parts_of(n):
                    lo, hi = rows_of(m)
                    expect(w.at[chunk_at(n), c, pl.ds(lo, hi - lo)], ag_r.at[ids[m]])
            forward(n)
        if ready:
            with jax.named_scope("fill#i=%d" % i):
                fill(i)
    for work in turns:
        work()
    for e in range(5):
        for a in range(2):
            if (a, e) not in done:
                project_block(a, e)

    gate = accp[:, 0:SEG]
    upper = accp[:, SEG:2 * SEG]
    grad_h = accp[:, 2 * SEG:]
    sig = 1.0 / (1.0 + jnp.exp(-gate))
    silu = gate * sig
    gg[:, 0:SEG] = (grad_h * upper * sig * (1.0 + gate * (1.0 - sig))).astype(BF16)
    gg[:, SEG:] = (grad_h * silu).astype(BF16)
    hp[...] = (silu * upper).astype(BF16)

    def weight_grad(ez):
        zb = at("z", -ez)
        if ez in EZ[:NZ - LATE]:
            turn(0, xpt, zb)
            turn(1, got, zb)
        gb[zb, :, :, :, 0:2 * SEG] = jnp.dot(xpt[zb], gg[...], preferred_element_type=F32).astype(BF16).reshape(
            NY, NC, HALF, 2 * SEG
        )
        gb[zb, :, :, :, 2 * SEG:] = jnp.dot(got[zb], hp[...], preferred_element_type=F32).astype(BF16).reshape(
            NY, NC, HALF, SEG
        )
        remote(gb.at[zb, :, 1 - c], gr.at[zb], gift_s, gift_r.at[EZ.index(ez)], {"c": 1 - c})

    gifted = set()

    def add_up(n, store):
        ez, _ = n
        if ez not in gifted:
            expect(gr.at[at("z", -ez)], gift_r.at[EZ.index(ez)])
            gifted.add(ez)
        kids = [(m, rows_of(m)) for m in sends_of(n)]
        for m, (a, b) in kids:
            expect(r.at[m[0] + 4, m[1] + 2, pl.ds(a, b - a)], rs_r.at[ids[m]])
        edges = sorted({0, HALF, *(v for _, ab in kids for v in ab)})
        zb, yb = at("z", -ez), at("y", -n[1])
        for a, b in zip(edges, edges[1:]):
            total = gb[zb, yb, c, a:b, :].astype(F32) + gr[zb, yb, a:b, :].astype(F32)
            for m, (ka, kb) in kids:
                if ka <= a and b <= kb:
                    total = total + r[m[0] + 4, m[1] + 2, a:b, :].astype(F32)
            store(a, b, total)

    def give(n):
        sz, sy = n[0] + 4, n[1] + 2

        def store(a, b, total):
            s[sz, sy, a:b, :] = total.astype(BF16)

        add_up(n, store)
        for m in parts_of(n):
            a, b = rows_of(m)
            axis, step = step_of(m)
            piece = s.at[sz, sy, pl.ds(a, b - a)]
            if m[1] == 0 and abs(m[0]) <= 2:
                side = 0 if m[0] > 0 else 1
                remote(piece, far_sum.at[side, c], back_s, top_r.at[side, c], {"z": at("z", -step), "c": par})
            else:
                remote(
                    piece, r.at[m[0] + 4, m[1] + 2, pl.ds(a, b - a)], rs_s, rs_r.at[ids[m]],
                    {axis: at(axis, -step)},
                )

    outs = []

    def share(which, left, lanes, zb):
        value = lax.dot_general(
            left[...], w[zb * NY:zb * NY + NY].reshape(ZB, WIDE)[:, lanes[0]:lanes[1]],
            (((1,), (1,)), ((), ())), preferred_element_type=F32,
        ).astype(BF16).reshape(NB, TOKENS, ZB)
        part[which, :, :, ZB * zb:ZB * zb + ZB] = value
        if zb == NZ - 1:
            over, under, across = at("x", 1), at("x", -1), at("x", 2)
            for i, (block, to) in enumerate((
                (across * NC, over), (over * NC + 1, over), (across * NC + 1, under), (under * NC, under),
            )):
                remote(part.at[which, block], ring.at[which, i], ring_s, ring_r.at[which, i], {"x": to})

    def share_on(which):
        for i, (at_ring, sign) in enumerate(((0, 1), (2, -1))):
            to = at("x", sign)
            expect(ring.at[which, at_ring], ring_r.at[which, at_ring])
            ringed[which, i] = (
                part[which, to * NC + i].astype(F32) + ring[which, at_ring].astype(F32)
            ).astype(BF16)
            remote(ringed.at[which, i], ring.at[which, 4 + i], ring_s, ring_r.at[which, 4 + i], {"x": to})

    def share_plane(which):
        for i in (1, 3, 4, 5):
            expect(ring.at[which, i], ring_r.at[which, i])
        for q, (i, k) in enumerate(((3, 4), (1, 5))):
            plane[which, q] = (
                part[which, x * NC + q].astype(F32) + ring[which, i].astype(F32) + ring[which, k].astype(F32)
            ).astype(BF16)

        @pl.when(moves)
        def _():
            for q in range(NC):
                remote(plane.at[which, q], crossed.at[which, 0], plane_s, plane_r.at[which, 0], {"z": zp, "c": q})

        @pl.when(keeps)
        def _():
            remote(plane.at[which, 1 - c], crossed.at[which, 1], plane_s, plane_r.at[which, 1], {"c": 1 - c})

    def put(src, dst, i):
        pltpu.make_async_copy(src, dst, out_s.at[i]).start()

    def share_final(which, out):
        expect(crossed.at[which, 0], plane_r.at[which, 0])

        @pl.when(keeps)
        def _():
            outv[which] = (plane[which, c].astype(F32) + crossed[which, 0].astype(F32)).astype(BF16)

        @pl.when(moves)
        def _():
            expect(crossed.at[which, 1], plane_r.at[which, 1])
            outv[which] = (crossed[which, 1].astype(F32) + crossed[which, 0].astype(F32)).astype(BF16)

        put(outv.at[which], out, which)

    def forward_gate():
        gate = accn[:, 0:SEG]
        upper = accn[:, SEG:]
        value = (gate * (1.0 / (1.0 + jnp.exp(-gate))) * upper).astype(BF16)
        hid[...] = value

        @pl.when(keeps)
        def _():
            put(hid, hid_ref, 2)

        @pl.when(moves)
        def _():
            remote(hid, hidv, hid_s, hid_r, {"z": zp, "c": 1 - c})

    def hidden_out():
        @pl.when(moves)
        def _():
            expect(hidv, hid_r)
            put(hidv, hid_ref, 2)

    def next_blocks(ezs):
        for ez in ezs:
            project(2, accn, (0, 2 * SEG), at("z", -ez), ez == 0)

    def share_in(zb):
        share(1, gg, (0, 2 * SEG), zb)

    def share_next(zb):
        share(0, hid, (2 * SEG, WIDE), zb)

    plan = [(3 + i // 2, share_in, i) for i in range(NZ)]
    plan += [(7, tok_far, 2), (7, next_blocks, EZ[0:4]), (8, next_blocks, EZ[4:8]), (9, forward_gate)]
    plan += [(10 + i // 2, share_next, i) for i in range(NZ - 1)]
    plan += [
        (13, share_on, 1), (13, share_next, NZ - 1), (20, share_plane, 1), (23, share_on, 0), (26, hidden_out),
        (29, share_plane, 0), (92, share_final, 1, gin_ref), (93, share_final, 0, out_ref),
    ]

    def between(until):
        while plan and plan[0][0] <= until:
            _, work, *given = plan.pop(0)
            with jax.named_scope("w#%s" % "_".join([work.__name__] + [str(v) for v in given if isinstance(v, int)])):
                work(*given)

    graded = set()
    for count, n in enumerate(REDUCE):
        for e in (abs(n[0]), abs(n[0]) - 1):
            if e >= 0 and e not in graded:
                with jax.named_scope("wgrad#e=%d" % e):
                    for ez in block_steps(e):
                        weight_grad(ez)
                graded.add(e)
        with jax.named_scope("give#i=%d#z=%d#y=%d" % (count, *n)):
            give(n)
        between(count + 1)

    with jax.named_scope("last"):

        @pl.when(moves)
        def _():
            home[...] = jnp.zeros((NC, HALF, WIDE), F32)

        def keep(a, b, total):
            home_in[0, a:b, :] = total.astype(BF16)

            @pl.when(keeps)
            def _():
                home[c, a:b, :] = total

        add_up((0, 0), keep)

        @pl.when(moves)
        def _():
            remote(home_in.at[0], home_in.at[1], home_s, home_r, {"c": 1 - c})

    between(99)
    with jax.named_scope("final"):

        @pl.when(keeps)
        def _():
            expect(home_in.at[1], home_r)
            home[1 - c] = home_in[1].astype(F32)

        for side in range(2):
            for q in range(NC):
                expect(far_sum.at[side, q], top_r.at[side, q])
        for q in range(NC):
            home[q] = (
                home[q] + far_sum[0, q].astype(F32) + far_sum[1, q].astype(F32)
            )
        put(home, wg_out, 3)
    with jax.named_scope("drain"):
        routed = sum(rows_of(m)[1] - rows_of(m)[0] for m in ids if m[1] or abs(m[0]) > 2) // HALF
        for count, sem in ((routed, ag_s), (routed, rs_s), (4, top_s), (4, back_s), (NZ * NY - 1, twin_s)):
            expect(w.at[pl.ds(0, count), 0], sem)
        expect(gr, gift_s)
        for count, sem in ((18, tk_s), (12, ring_s)):
            expect(tok.at[pl.ds(0, count)], sem)

        @pl.when(keeps)
        def _():
            expect(own, home_s)
            expect(tok.at[pl.ds(0, 3)], hop_s)
            expect(tok.at[pl.ds(0, 2)], plane_s)

        @pl.when(moves)
        def _():
            expect(home_in.at[0], home_s)
            expect(tok.at[pl.ds(0, 6)], hop_s)
            expect(tok.at[pl.ds(0, 4)], plane_s)
            expect(hid, hid_s)

        for i, (src, dst) in enumerate(((outv.at[0], out_ref), (outv.at[1], gin_ref), (hid, hid_ref), (home, wg_out))):
            pltpu.make_async_copy(src, dst, out_s.at[i]).wait()


def finish(
    factor, out_in, hid_in, gin_in, wg_in, ag_in, au_in, ad_in,
    out_ref, hid_ref, gin_ref, ng_ref, nu_ref, nd_ref, hidv, wg, ag, au, ad, sems,
):
    pairs = ((wg_in, wg), (out_in, out_ref), (gin_in, gin_ref), (hid_in, hidv), (ag_in, ag), (au_in, au), (ad_in, ad))
    copies = [pltpu.make_async_copy(src, dst, sems.at[i]) for i, (src, dst) in enumerate(pairs)]
    for copy in copies:
        copy.start()
    for copy in copies:
        copy.wait()
    hid_ref[...] = hidv[:, 0:UNITS]
    for i, (acc, new) in enumerate(((ag, ng_ref), (au, nu_ref), (ad, nd_ref))):
        for q in range(NC):
            half = slice(HALF * q, HALF * q + HALF)
            new[half, :] = acc[half, :] + factor * wg[q, :, SEG * i:SEG * i + UNITS]


def local(x_next, x_prev, grad_out, gate_w, up_w, down_w, acc_gate, acc_up, acc_down):
    _, ids = gather_plan()
    vmem = pl.BlockSpec(memory_space=pltpu.VMEM)
    hbm = pl.BlockSpec(memory_space=pl.ANY)
    dma = pltpu.SemaphoreType.DMA
    total_rows = x_prev.shape[0] * NZ * NY * NX * NC
    factor = 1.0 / math.sqrt(total_rows)
    rows = jax.ShapeDtypeStruct((TOKENS, 2048), BF16)
    out_next, hidden, grad_input, grads = pl.pallas_call(
        layer,
        out_shape=(
            rows, jax.ShapeDtypeStruct((GROUP, SEG), BF16), rows, jax.ShapeDtypeStruct((NC, HALF, WIDE), F32),
        ),
        in_specs=[hbm] * 6,
        out_specs=(hbm,) * 4,
        scratch_shapes=[
            pltpu.VMEM((3, TOKENS, 2048), BF16),
            pltpu.VMEM((3, ROWS, UNITS), BF16),
            pltpu.VMEM((NC, HALF, WIDE), BF16),
            pltpu.VMEM((NZ * NY, NC, HALF, WIDE), BF16),
            pltpu.VMEM((3 * NB, TOKENS, 2048), BF16),
            pltpu.VMEM((NZ, ZB, GROUP), BF16),
            pltpu.VMEM((NZ, ZB, GROUP), BF16),
            pltpu.VMEM((GROUP, WIDE), F32),
            pltpu.VMEM((GROUP, 2 * SEG), F32),
            pltpu.VMEM((GROUP, 2 * SEG), BF16),
            pltpu.VMEM((GROUP, SEG), BF16),
            pltpu.VMEM((GROUP, SEG), BF16),
            pltpu.VMEM((GROUP, SEG), BF16),
            pltpu.VMEM((NZ, NY, NC, HALF, WIDE), BF16),
            pltpu.VMEM((NZ, NY, HALF, WIDE), BF16),
            pltpu.VMEM((9, 5, HALF, WIDE), BF16),
            pltpu.VMEM((9, 5, HALF, WIDE), BF16),
            pltpu.VMEM((2, NC, HALF, WIDE), BF16),
            pltpu.VMEM((2, HALF, WIDE), BF16),
            pltpu.VMEM((NC, HALF, WIDE), F32),
            pltpu.VMEM((2, NB, TOKENS, 2048), BF16),
            pltpu.VMEM((2, 6, TOKENS, 2048), BF16),
            pltpu.VMEM((2, 2, TOKENS, 2048), BF16),
            pltpu.VMEM((2, NC, TOKENS, 2048), BF16),
            pltpu.VMEM((2, NC, TOKENS, 2048), BF16),
            pltpu.VMEM((2, TOKENS, 2048), BF16),
            dma, dma((len(ids),)), dma, dma, dma, dma((len(EZ),)), dma, dma((3, NC)), dma, dma((3, 4)),
            dma, dma((len(EZ),)), dma, dma((len(ids),)), dma, dma((2, NC)), dma, dma,
            dma, dma((2, 6)), dma, dma((2, 2)),
            dma, dma, dma((4,)), dma((6,)),
        ],
        compiler_params=pltpu.CompilerParams(
            collective_id=0, has_side_effects=True, vmem_limit_bytes=60 * 1024 * 1024
        ),
        name="layer",
    )(x_next, x_prev, grad_out, gate_w, up_w, down_w.T)
    sums = jax.ShapeDtypeStruct((ROWS, UNITS), F32)
    out_next, hidden, grad_input, new_gate, new_up, new_down = pl.pallas_call(
        functools.partial(finish, factor),
        out_shape=(rows, jax.ShapeDtypeStruct((GROUP, UNITS), BF16), rows, sums, sums, sums),
        in_specs=[hbm] * 7,
        out_specs=(vmem,) * 6,
        scratch_shapes=[pltpu.VMEM((GROUP, SEG), BF16), pltpu.VMEM((NC, HALF, WIDE), F32)]
        + [pltpu.VMEM((ROWS, UNITS), F32)] * 3 + [dma((7,))],
        compiler_params=pltpu.CompilerParams(vmem_limit_bytes=60 * 1024 * 1024),
        name="finish",
    )(out_next, hidden, grad_input, grads, acc_gate, acc_up, acc_down.T)
    return out_next, hidden, grad_input, new_gate, new_up, new_down.T


def solution(mesh):
    split = Mesh(mesh.devices.reshape(NZ, NY, NX, NC), ("z", "y", "x", "c"))
    in_specs = (
        P(TOK, None), P(TOK, None), P(TOK, None),
        P(FS, TP), P(FS, TP), P(TP, FS), P(FS, TP), P(FS, TP), P(TP, FS),
    )
    out_specs = (P(TOK, None), P(FS, TP), P(TOK, None), P(FS, TP), P(FS, TP), P(TP, FS))
    return jax.shard_map(local, mesh=split, in_specs=in_specs, out_specs=out_specs, check_vma=False)
```

time: 284 us -> 72.3 us (0.25)
  waiting for transfers between devices: 192 us -> 0 us
  Pallas kernels: 0 us -> 71.6 us
  matrix products: 27.5 us -> 0 us
  blocking collectives: 20.6 us -> 0 us
  starting transfers between devices: 14.5 us -> 0 us
  between operations: 13.9 us -> 0.64 us
  other arithmetic: 7.99 us -> 0 us
  local copies, waits for them, and re-layouts: 5.77 us -> 0 us
    all_gather x2 -> x0, waiting for transfers between devices: 113 us -> none  [the longest x1 82.3 us: turned_gather(): lax.all_gather(both, axis, axis=0, tiled=True)]
    all_to_all x3 -> x0, waiting for transfers between devices: 77.7 us -> none  [the longest x1 62.3 us: sum_at_owner(): lax.all_to_all(cut_along(array, dim, length), axis, 0, 0, tiled=True)]
    pallas_call x0 -> x2, Pallas kernels: none -> 71.6 us  [the longest x1 69.5 us: local(): pl.pallas_call(layer, out_shape=(rows, jax.ShapeDtypeStruct((GROUP, SEG),...]
    dot_general x10 -> x0, matrix products: 27.5 us -> none  [the longest x3 8.04 us: contract_cols(): lax.dot_general(left, right, (((1,), (1,)), ((), ())), preferred_element_...]
    all_to_all x1 -> x0, blocking collectives: 20.6 us -> none  [sent_to_all(): lax.all_to_all(jnp.broadcast_to(array[None], (length, *array.shape)), axi...]
    all_to_all x3 -> x0, starting transfers between devices: 14.3 us -> none  [the longest x2 8.84 us: summed_on_arrival(): lax.all_to_all(blocks, axis, split_axis=0, concat_axis=0, tiled=True)]
    unnamed x19 -> x0, local copies, waits for them, and re-layouts: 4.06 us -> none
    reduce_sum x3 -> x0, other arithmetic: 3.99 us -> none  [the longest x2 3.81 us: summed_on_arrival(): return arrived.astype(jnp.float32).sum(axis=0)]
  transfers between devices with their start and end apart: 7 -> 0, of which waited for: 6 -> 0; matrix products, arithmetic and copies ran while one was open for 9% -> 0% of each run, Pallas kernels for 0% -> 0%
where the time goes in v1:
time: 72.3 us; the launch traced here: 72.2 us
  Pallas kernels  71.6 us (99%)
    pallas_call x1, Pallas kernels, local(): pl.pallas_call(layer, out_shape=(rows, jax.ShapeDtypeStruct((GROUP, SEG),...  69.5 us
    pallas_call x1, Pallas kernels, local(): pl.pallas_call(functools.partial(finish, factor), out_shape=(rows, jax.Sh...  2.09 us

profile of v1, /device:TPU:1, one launch (start us, length us, event | category | flops | bytes accessed | tf_op | source)
XLA Modules:
  0.0 72.2 jit_solution(5092726387272678040)
XLA Ops:
  0.6 69.5 %layer.1 = (bf16[24,2048]{1,0:T(8,128)(2,1)}, bf16[192,384]{1,0:T(8,128)(2,1)}, bf16[24,2048]{1,0:T(8,128)(2,1)}, f32[2,32,1152]{2,1,0:T(8,128)}) custom-call(bf16[24,2048]{1,0:T(8,128)(2,1)} %xn_in.1, bf16[24,2048]{1,0:T(8,128)(2,1)} %xp_in.1, bf16[24,2048]{1,0:T(8,128)(2,1)} %go_in.1, bf16[64,352]{1,0:T(8,128)(2,1)} %gw_in.1, bf16[64,352]{1,0:T(8,128)(2,1)} %uw_in.1, ...), custom_call_target="tpu_custom_call" | custom-call | tf_op jit(solution)/shard_map/layer/pallas_call | solution.py:606
  70.1 2.1 %finish.1 = (bf16[24,2048]{1,0:T(8,128)(2,1)}, bf16[192,352]{1,0:T(8,128)(2,1)}, bf16[24,2048]{1,0:T(8,128)(2,1)}, f32[64,352]{1,0:T(8,128)}, f32[64,352]{1,0:T(8,128)}, /*index=5*/f32[64,352]{1,0:T(8,128)}) custom-call(bf16[24,2048]{1,0:T(8,128)(2,1)} %get-tuple-element.16.out_in, bf16[192,384]{1,0:T(8,128)(2,1)} %get-tuple-element.17.hid_in, ...), custom_call_target="tpu_custom_call" | custom-call | tf_op jit(solution)/shard_map/finish/pallas_call | solution.py:651

commit v2 on v1

--- a/solution.py
+++ b/solution.py
@@ -16,32 +16,32 @@
 FS, TP = ("z", "y"), ("x", "c")
 NZ, NY, NX, NC = 8, 4, 4, 2
 NB = NX * NC
+PACK = 264
 ROWS, HALF = 64, 32
 UNITS = 352
 SEG = 384
-WIDE = 3 * SEG
 ZB = NY * ROWS
 TOKENS = 24
 GROUP = NB * TOKENS
 LATE = 5
-LATENCY, ROW_US = 1.8, 1.0 / 20.2
+LATENCY, ROW_US = 1.8, 1.45 / 264
 
 EZ = (0, 1, -1, 2, -2, 3, -3, 4)
 EY = (0, 1, -1, 2)
 REDUCE = (
-    (4, 2), (3, 2), (-3, 2), (-2, 2), (4, -1), (4, 1), (3, -1), (-1, 2), (2, 2), (-3, -1), (3, 1), (-3, 1), (-2, -1),
-    (1, 2), (-2, 1), (4, 0), (2, -1), (2, 1), (0, 2), (-3, 0), (3, 0), (-1, 1), (-1, -1), (-2, 0), (1, -1), (2, 0),
-    (1, 1), (0, -1), (0, 1), (-1, 0), (1, 0),
+    (4, 2), (3, 2), (-3, 2), (-2, 2), (2, 2), (4, -1), (4, 1), (-1, 2), (3, -1), (3, 1), (1, 2), (-3, -1), (-3, 1),
+    (0, 2), (-2, -1), (-2, 1), (2, -1), (2, 1), (4, 0), (-1, -1), (-1, 1), (3, 0), (-3, 0), (1, -1), (1, 1), (0, -1),
+    (0, 1), (-2, 0), (2, 0), (-1, 0), (1, 0),
 )
 
 
 def rows_of(m):
     ez, ey = m
     if abs(ey) == 2:
-        return (0, HALF // 2) if ey > 0 else (HALF // 2, HALF)
+        return (0, 128) if ey > 0 else (128, PACK)
     if ey == 0 and abs(ez) == 4:
-        return (0, HALF // 2) if ez > 0 else (HALF // 2, HALF)
-    return 0, HALF
+        return (0, 128) if ez > 0 else (128, PACK)
+    return 0, PACK
 
 
 def sends_of(n):
@@ -75,6 +75,39 @@
     return "z", (1 if abs(ez) == 1 else 2) * (1 if ez > 0 else -1)
 
 
+def widened(v, lanes):
+    return jnp.concatenate([v, jnp.zeros((v.shape[0], lanes - v.shape[1]), v.dtype)], axis=1)
+
+
+def known(v):
+    v = v[:, 0:SEG]
+    return jnp.where(lax.broadcasted_iota(jnp.int32, v.shape, 1) < UNITS, v, 0.0)
+
+
+def packed_pair(gate, upper):
+    both = pltpu.roll(widened(upper, 512), 96, 1)
+    return jnp.concatenate([gate[:, 0:256], gate[:, 256:384] + both[:, 0:128], both[:, 128:512]], axis=1)
+
+
+def packed_last(down):
+    return pltpu.roll(widened(down, 512), 64, 1)
+
+
+def folded(v):
+    v = v.reshape(v.shape[0] // HALF, 4, 8, 128)
+    total = v[:, 0].reshape(-1, 128)
+    for k in range(1, 4):
+        total = total + pltpu.roll(v[:, k].reshape(-1, 128), 32 * k, 1)
+    return total
+
+
+def unfolded(v):
+    n = v.shape[0] // 8
+    keep = lax.broadcasted_iota(jnp.int32, v.shape, 1) < 32
+    parts = [jnp.where(keep, v if k == 0 else pltpu.roll(v, 128 - 32 * k, 1), 0.0).reshape(n, 1, 8, 128) for k in range(4)]
+    return jnp.concatenate(parts, axis=1).reshape(HALF * n, 128)
+
+
 @functools.lru_cache
 def gather_plan():
     free, heap, got, order, ends = {}, [], set(), [], {}
@@ -82,7 +115,7 @@
     def push(now, m):
         axis, step = step_of(m)
         lo, hi = rows_of(m)
-        cost = (hi - lo) * ROW_US * abs(step) if abs(m[0]) > 2 or m[1] else HALF * ROW_US * abs(step)
+        cost = (hi - lo) * ROW_US * abs(step) if abs(m[0]) > 2 or m[1] else PACK * ROW_US * abs(step)
         link = axis, step > 0
         free[link] = max(now, free.get(link, 0.0)) + cost
         ends[m] = free[link]
@@ -111,7 +144,7 @@
 def layer(
     xn_in, xp_in, go_in, gw_in, uw_in, dw_in,
     out_ref, hid_ref, gin_ref, wg_out,
-    mine, ours, own, w, tok, xpt, got, accp, accn, gg, hp, hid, hidv, gb, gr, s, r, far_sum, home_in, home,
+    mine, ours, own, w, tok, xpt, got, accp, accd, accn, gg, hp, hid, hidp, hidv, gb, gr, s, r, far_sum, home_in, home,
     part, ring, ringed, plane, crossed, outv,
     ag_s, ag_r, home_s, home_r, twin_s, twin_r, hop_s, hop_r, tk_s, tk_r,
     gift_s, gift_r, rs_s, rs_r, top_s, top_r, back_s, back_r, ring_s, ring_r, plane_s, plane_r,
@@ -142,12 +175,22 @@
     for copy in loads:
         copy.start()
 
-    own[...] = jnp.zeros((NC, HALF, WIDE), BF16)
     for copy in loads:
         copy.wait()
+
+    gate_up_down = [widened(ours[i].astype(F32), SEG) for i in range(3)]
+    pair = packed_pair(*gate_up_down[0:2])
+    last = packed_last(gate_up_down[2])
     for q in range(NC):
-        for i in range(3):
-            own[q, :, SEG * i:SEG * i + UNITS] = ours[i, HALF * q:HALF * q + HALF, :]
+        rows = slice(HALF * q, HALF * q + HALF)
+        for t in range(8):
+            column = jnp.zeros((HALF, 128), F32)
+            if t < 6:
+                column = column + pair[rows, 128 * t:128 * t + 128]
+            if t > 4:
+                column = column + last[rows, 128 * (t - 5):128 * (t - 4)]
+            own[q, HALF * t:HALF * t + HALF, :] = column.astype(BF16)
+        own[q, 256:PACK, :] = folded(last[rows, 384:512]).astype(BF16)
 
     @pl.when(keeps)
     def _():
@@ -261,8 +304,12 @@
     def cols(zb):
         return pl.ds(pl.multiple_of(zb * ZB, ZB), ZB)
 
-    def weights(zb):
-        return w[pl.ds(zb * NY, NY)].reshape(ZB, WIDE)
+    def weights(zb, first, end):
+        parts = [w[pl.ds(zb * NY, NY), :, HALF * t:HALF * t + HALF, :].reshape(ZB, 128) for t in range(first, min(end, 8))]
+        if end > 8:
+            tail = w[pl.ds(zb * NY, NY), :, 256:PACK, :].astype(F32).reshape(NY * NC * 8, 128)
+            parts.append(unfolded(tail).astype(BF16))
+        return jnp.concatenate(parts, axis=1)
 
     eye_zb = (
         lax.broadcasted_iota(jnp.int32, (ZB, ZB), 0) == lax.broadcasted_iota(jnp.int32, (ZB, ZB), 1)
@@ -274,13 +321,13 @@
             eye_zb, block, (((1,), (1,)), ((), ())), preferred_element_type=F32
         ).astype(BF16)
 
-    def project(a, acc, lanes, zb, first):
+    def project(a, acc, columns, zb, first):
         block = tok[NB * a:NB * a + NB, :, cols(zb)].reshape(GROUP, ZB)
-        value = jnp.dot(block, weights(zb)[:, lanes[0]:lanes[1]], preferred_element_type=F32)
+        value = jnp.dot(block, weights(zb, *columns), preferred_element_type=F32)
         if first:
-            acc[:, lanes[0]:lanes[1]] = value
+            acc[...] = value
         else:
-            acc[:, lanes[0]:lanes[1]] += value
+            acc[...] += value
 
     def block_steps(e):
         return (e,) if e in (0, 4) else (e, -e)
@@ -294,7 +341,7 @@
                 count = NY - 1 if ez == 0 else NY
                 expect(w.at[pl.ds(0, count), 1 - c], twin_r.at[EZ.index(ez)])
                 twins.add(ez)
-            project(a, accp, ((0, 2 * SEG), (2 * SEG, WIDE))[a], at("z", -ez), ez == 0)
+            project(a, (accp, accd)[a], ((0, 6), (5, 9))[a], at("z", -ez), ez == 0)
         done.add((a, e))
 
     twins, ready = set(), set()
@@ -343,26 +390,32 @@
             if (a, e) not in done:
                 project_block(a, e)
 
-    gate = accp[:, 0:SEG]
-    upper = accp[:, SEG:2 * SEG]
-    grad_h = accp[:, 2 * SEG:]
+    gate = known(accp[...])
+    upper = known(pltpu.roll(accp[...], 768 - UNITS, 1))
+    grad_h = known(pltpu.roll(accd[...], 448, 1))
     sig = 1.0 / (1.0 + jnp.exp(-gate))
     silu = gate * sig
-    gg[:, 0:SEG] = (grad_h * upper * sig * (1.0 + gate * (1.0 - sig))).astype(BF16)
-    gg[:, SEG:] = (grad_h * silu).astype(BF16)
-    hp[...] = (silu * upper).astype(BF16)
+    gg[...] = packed_pair(
+        grad_h * upper * sig * (1.0 + gate * (1.0 - sig)), grad_h * silu
+    ).astype(BF16)
+    hp[...] = packed_last(silu * upper).astype(BF16)
 
     def weight_grad(ez):
         zb = at("z", -ez)
         if ez in EZ[:NZ - LATE]:
             turn(0, xpt, zb)
             turn(1, got, zb)
-        gb[zb, :, :, :, 0:2 * SEG] = jnp.dot(xpt[zb], gg[...], preferred_element_type=F32).astype(BF16).reshape(
-            NY, NC, HALF, 2 * SEG
-        )
-        gb[zb, :, :, :, 2 * SEG:] = jnp.dot(got[zb], hp[...], preferred_element_type=F32).astype(BF16).reshape(
-            NY, NC, HALF, SEG
-        )
+        pair = jnp.dot(xpt[zb], gg[...], preferred_element_type=F32)
+        last = jnp.dot(got[zb], hp[...], preferred_element_type=F32)
+        for t in range(8):
+            if t < 5:
+                column = pair[:, 128 * t:128 * t + 128]
+            elif t == 5:
+                column = pair[:, 640:768] + last[:, 0:128]
+            else:
+                column = last[:, 128 * (t - 5):128 * (t - 4)]
+            gb[zb, :, :, HALF * t:HALF * t + HALF, :] = column.astype(BF16).reshape(NY, NC, HALF, 128)
+        gb[zb, :, :, 256:PACK, :] = folded(last[:, 384:512]).astype(BF16).reshape(NY, NC, 8, 128)
         remote(gb.at[zb, :, 1 - c], gr.at[zb], gift_s, gift_r.at[EZ.index(ez)], {"c": 1 - c})
 
     gifted = set()
@@ -375,7 +428,7 @@
         kids = [(m, rows_of(m)) for m in sends_of(n)]
         for m, (a, b) in kids:
             expect(r.at[m[0] + 4, m[1] + 2, pl.ds(a, b - a)], rs_r.at[ids[m]])
-        edges = sorted({0, HALF, *(v for _, ab in kids for v in ab)})
+        edges = sorted({0, PACK, *(v for _, ab in kids for v in ab)})
         zb, yb = at("z", -ez), at("y", -n[1])
         for a, b in zip(edges, edges[1:]):
             total = gb[zb, yb, c, a:b, :].astype(F32) + gr[zb, yb, a:b, :].astype(F32)
@@ -406,50 +459,67 @@
 
     outs = []
 
-    def share(which, left, lanes, zb):
+    def share(which, left, columns, zb):
         value = lax.dot_general(
-            left[...], w[zb * NY:zb * NY + NY].reshape(ZB, WIDE)[:, lanes[0]:lanes[1]],
+            left[...], weights(zb, *columns),
             (((1,), (1,)), ((), ())), preferred_element_type=F32,
         ).astype(BF16).reshape(NB, TOKENS, ZB)
         part[which, :, :, ZB * zb:ZB * zb + ZB] = value
-        if zb == NZ - 1:
+        if zb % 4 == 3:
+            h = zb // 4
             over, under, across = at("x", 1), at("x", -1), at("x", 2)
             for i, (block, to) in enumerate((
                 (across * NC, over), (over * NC + 1, over), (across * NC + 1, under), (under * NC, under),
             )):
-                remote(part.at[which, block], ring.at[which, i], ring_s, ring_r.at[which, i], {"x": to})
-
-    def share_on(which):
+                remote(
+                    part.at[which, block, :, wide[h]], ring.at[which, i, :, wide[h]],
+                    ring_s, ring_r.at[which, h, i], {"x": to},
+                )
+
+    wide = (pl.ds(0, 1024), pl.ds(1024, 1024))
+
+    def share_on(which, h):
         for i, (at_ring, sign) in enumerate(((0, 1), (2, -1))):
             to = at("x", sign)
-            expect(ring.at[which, at_ring], ring_r.at[which, at_ring])
-            ringed[which, i] = (
-                part[which, to * NC + i].astype(F32) + ring[which, at_ring].astype(F32)
+            expect(ring.at[which, at_ring, :, wide[h]], ring_r.at[which, h, at_ring])
+            ringed[which, i, :, wide[h]] = (
+                part[which, to * NC + i, :, wide[h]].astype(F32) + ring[which, at_ring, :, wide[h]].astype(F32)
             ).astype(BF16)
-            remote(ringed.at[which, i], ring.at[which, 4 + i], ring_s, ring_r.at[which, 4 + i], {"x": to})
-
-    def share_plane(which):
+            remote(
+                ringed.at[which, i, :, wide[h]], ring.at[which, 4 + i, :, wide[h]],
+                ring_s, ring_r.at[which, h, 4 + i], {"x": to},
+            )
+
+    def share_plane(which, h):
         for i in (1, 3, 4, 5):
-            expect(ring.at[which, i], ring_r.at[which, i])
+            expect(ring.at[which, i, :, wide[h]], ring_r.at[which, h, i])
         for q, (i, k) in enumerate(((3, 4), (1, 5))):
-            plane[which, q] = (
-                part[which, x * NC + q].astype(F32) + ring[which, i].astype(F32) + ring[which, k].astype(F32)
+            plane[which, q, :, wide[h]] = (
+                part[which, x * NC + q, :, wide[h]].astype(F32)
+                + ring[which, i, :, wide[h]].astype(F32) + ring[which, k, :, wide[h]].astype(F32)
             ).astype(BF16)
 
         @pl.when(moves)
         def _():
             for q in range(NC):
-                remote(plane.at[which, q], crossed.at[which, 0], plane_s, plane_r.at[which, 0], {"z": zp, "c": q})
+                remote(
+                    plane.at[which, q, :, wide[h]], crossed.at[which, 0, :, wide[h]],
+                    plane_s, plane_r.at[which, h, 0], {"z": zp, "c": q},
+                )
 
         @pl.when(keeps)
         def _():
-            remote(plane.at[which, 1 - c], crossed.at[which, 1], plane_s, plane_r.at[which, 1], {"c": 1 - c})
+            remote(
+                plane.at[which, 1 - c, :, wide[h]], crossed.at[which, 1, :, wide[h]],
+                plane_s, plane_r.at[which, h, 1], {"c": 1 - c},
+            )
 
     def put(src, dst, i):
         pltpu.make_async_copy(src, dst, out_s.at[i]).start()
 
     def share_final(which, out):
-        expect(crossed.at[which, 0], plane_r.at[which, 0])
+        for h in range(2):
+            expect(crossed.at[which, 0, :, wide[h]], plane_r.at[which, h, 0])
 
         @pl.when(keeps)
         def _():
@@ -457,16 +527,18 @@
 
         @pl.when(moves)
         def _():
-            expect(crossed.at[which, 1], plane_r.at[which, 1])
+            for h in range(2):
+                expect(crossed.at[which, 1, :, wide[h]], plane_r.at[which, h, 1])
             outv[which] = (crossed[which, 1].astype(F32) + crossed[which, 0].astype(F32)).astype(BF16)
 
         put(outv.at[which], out, which)
 
     def forward_gate():
-        gate = accn[:, 0:SEG]
-        upper = accn[:, SEG:]
-        value = (gate * (1.0 / (1.0 + jnp.exp(-gate))) * upper).astype(BF16)
-        hid[...] = value
+        gate = known(accn[...])
+        upper = known(pltpu.roll(accn[...], 768 - UNITS, 1))
+        value = gate * (1.0 / (1.0 + jnp.exp(-gate))) * upper
+        hid[...] = value.astype(BF16)
+        hidp[...] = packed_last(value).astype(BF16)
 
         @pl.when(keeps)
         def _():
@@ -484,20 +556,22 @@
 
     def next_blocks(ezs):
         for ez in ezs:
-            project(2, accn, (0, 2 * SEG), at("z", -ez), ez == 0)
+            project(2, accn, (0, 6), at("z", -ez), ez == 0)
 
     def share_in(zb):
-        share(1, gg, (0, 2 * SEG), zb)
+        share(1, gg, (0, 6), zb)
 
     def share_next(zb):
-        share(0, hid, (2 * SEG, WIDE), zb)
-
-    plan = [(3 + i // 2, share_in, i) for i in range(NZ)]
+        share(0, hidp, (5, 9), zb)
+
+    plan = [(0, share_in, 0)] + [(3 + (i - 1) // 2, share_in, i) for i in range(1, NZ)]
     plan += [(7, tok_far, 2), (7, next_blocks, EZ[0:4]), (8, next_blocks, EZ[4:8]), (9, forward_gate)]
-    plan += [(10 + i // 2, share_next, i) for i in range(NZ - 1)]
+    plan += [(9, share_next, 0), (9, share_on, 1, 0), (10, share_next, 1), (10, share_next, 2), (11, share_next, 3)]
+    plan += [(11, share_next, 4), (12, share_next, 5), (12, share_on, 1, 1), (13, share_next, 6), (13, share_next, 7)]
     plan += [
-        (13, share_on, 1), (13, share_next, NZ - 1), (20, share_plane, 1), (23, share_on, 0), (26, hidden_out),
-        (29, share_plane, 0), (92, share_final, 1, gin_ref), (93, share_final, 0, out_ref),
+        (19, share_plane, 1, 0), (22, share_on, 0, 0), (23, share_plane, 1, 1), (26, share_on, 0, 1),
+        (27, hidden_out), (28, share_plane, 0, 0), (29, share_plane, 0, 1),
+        (92, share_final, 1, gin_ref), (93, share_final, 0, out_ref),
     ]
 
     def between(until):
@@ -514,6 +588,7 @@
                     for ez in block_steps(e):
                         weight_grad(ez)
                 graded.add(e)
+        between(count)
         with jax.named_scope("give#i=%d#z=%d#y=%d" % (count, *n)):
             give(n)
         between(count + 1)
@@ -522,7 +597,7 @@
 
         @pl.when(moves)
         def _():
-            home[...] = jnp.zeros((NC, HALF, WIDE), F32)
+            home[...] = jnp.zeros((NC, PACK, 128), F32)
 
         def keep(a, b, total):
             home_in[0, a:b, :] = total.astype(BF16)
@@ -554,7 +629,7 @@
             )
         put(home, wg_out, 3)
     with jax.named_scope("drain"):
-        routed = sum(rows_of(m)[1] - rows_of(m)[0] for m in ids if m[1] or abs(m[0]) > 2) // HALF
+        routed = sum(rows_of(m)[1] - rows_of(m)[0] for m in ids if m[1] or abs(m[0]) > 2) // PACK
         for count, sem in ((routed, ag_s), (routed, rs_s), (4, top_s), (4, back_s), (NZ * NY - 1, twin_s)):
             expect(w.at[pl.ds(0, count), 0], sem)
         expect(gr, gift_s)
@@ -589,10 +664,15 @@
     for copy in copies:
         copy.wait()
     hid_ref[...] = hidv[:, 0:UNITS]
-    for i, (acc, new) in enumerate(((ag, ng_ref), (au, nu_ref), (ad, nd_ref))):
-        for q in range(NC):
-            half = slice(HALF * q, HALF * q + HALF)
-            new[half, :] = acc[half, :] + factor * wg[q, :, SEG * i:SEG * i + UNITS]
+    for q in range(NC):
+        column = [wg[q, HALF * t:HALF * t + HALF, :] for t in range(8)]
+        tail = unfolded(wg[q, 256:PACK, :])
+        gate = jnp.concatenate(column[0:3], axis=1)
+        upper = pltpu.roll(jnp.concatenate(column[2:6], axis=1), 416, 1)
+        down = pltpu.roll(jnp.concatenate(column[5:8] + [tail], axis=1), 448, 1)
+        half = slice(HALF * q, HALF * q + HALF)
+        for acc, new, value in ((ag, ng_ref, gate), (au, nu_ref, upper), (ad, nd_ref, down)):
+            new[half, :] = acc[half, :] + factor * value[:, 0:UNITS]
 
 
 def local(x_next, x_prev, grad_out, gate_w, up_w, down_w, acc_gate, acc_up, acc_down):
@@ -606,31 +686,33 @@
     out_next, hidden, grad_input, grads = pl.pallas_call(
         layer,
         out_shape=(
-            rows, jax.ShapeDtypeStruct((GROUP, SEG), BF16), rows, jax.ShapeDtypeStruct((NC, HALF, WIDE), F32),
+            rows, jax.ShapeDtypeStruct((GROUP, SEG), BF16), rows, jax.ShapeDtypeStruct((NC, PACK, 128), F32),
         ),
         in_specs=[hbm] * 6,
         out_specs=(hbm,) * 4,
         scratch_shapes=[
             pltpu.VMEM((3, TOKENS, 2048), BF16),
             pltpu.VMEM((3, ROWS, UNITS), BF16),
-            pltpu.VMEM((NC, HALF, WIDE), BF16),
-            pltpu.VMEM((NZ * NY, NC, HALF, WIDE), BF16),
+            pltpu.VMEM((NC, PACK, 128), BF16),
+            pltpu.VMEM((NZ * NY, NC, PACK, 128), BF16),
             pltpu.VMEM((3 * NB, TOKENS, 2048), BF16),
             pltpu.VMEM((NZ, ZB, GROUP), BF16),
             pltpu.VMEM((NZ, ZB, GROUP), BF16),
-            pltpu.VMEM((GROUP, WIDE), F32),
+            pltpu.VMEM((GROUP, 768), F32),
+            pltpu.VMEM((GROUP, 512), F32),
             pltpu.VMEM((GROUP, 2 * SEG), F32),
             pltpu.VMEM((GROUP, 2 * SEG), BF16),
+            pltpu.VMEM((GROUP, 512), BF16),
             pltpu.VMEM((GROUP, SEG), BF16),
+            pltpu.VMEM((GROUP, 512), BF16),
             pltpu.VMEM((GROUP, SEG), BF16),
-            pltpu.VMEM((GROUP, SEG), BF16),
-            pltpu.VMEM((NZ, NY, NC, HALF, WIDE), BF16),
-            pltpu.VMEM((NZ, NY, HALF, WIDE), BF16),
-            pltpu.VMEM((9, 5, HALF, WIDE), BF16),
-            pltpu.VMEM((9, 5, HALF, WIDE), BF16),
-            pltpu.VMEM((2, NC, HALF, WIDE), BF16),
-            pltpu.VMEM((2, HALF, WIDE), BF16),
-            pltpu.VMEM((NC, HALF, WIDE), F32),
+            pltpu.VMEM((NZ, NY, NC, PACK, 128), BF16),
+            pltpu.VMEM((NZ, NY, PACK, 128), BF16),
+            pltpu.VMEM((9, 5, PACK, 128), BF16),
+            pltpu.VMEM((9, 5, PACK, 128), BF16),
+            pltpu.VMEM((2, NC, PACK, 128), BF16),
+            pltpu.VMEM((2, PACK, 128), BF16),
+            pltpu.VMEM((NC, PACK, 128), F32),
             pltpu.VMEM((2, NB, TOKENS, 2048), BF16),
             pltpu.VMEM((2, 6, TOKENS, 2048), BF16),
             pltpu.VMEM((2, 2, TOKENS, 2048), BF16),
@@ -639,7 +721,7 @@
             pltpu.VMEM((2, TOKENS, 2048), BF16),
             dma, dma((len(ids),)), dma, dma, dma, dma((len(EZ),)), dma, dma((3, NC)), dma, dma((3, 4)),
             dma, dma((len(EZ),)), dma, dma((len(ids),)), dma, dma((2, NC)), dma, dma,
-            dma, dma((2, 6)), dma, dma((2, 2)),
+            dma, dma((2, 2, 6)), dma, dma((2, 2, 2)),
             dma, dma, dma((4,)), dma((6,)),
         ],
         compiler_params=pltpu.CompilerParams(
@@ -653,7 +735,7 @@
         out_shape=(rows, jax.ShapeDtypeStruct((GROUP, UNITS), BF16), rows, sums, sums, sums),
         in_specs=[hbm] * 7,
         out_specs=(vmem,) * 6,
-        scratch_shapes=[pltpu.VMEM((GROUP, SEG), BF16), pltpu.VMEM((NC, HALF, WIDE), F32)]
+        scratch_shapes=[pltpu.VMEM((GROUP, SEG), BF16), pltpu.VMEM((NC, PACK, 128), F32)]
         + [pltpu.VMEM((ROWS, UNITS), F32)] * 3 + [dma((7,))],
         compiler_params=pltpu.CompilerParams(vmem_limit_bytes=60 * 1024 * 1024),
         name="finish",

time: 72.3 us -> 68.9 us (0.953)
  Pallas kernels: 71.6 us -> 68.1 us
    pallas_call x1, Pallas kernels: 69.5 us -> 66 us  [local(): pl.pallas_call(layer, out_shape=(rows, jax.ShapeDtypeStruct((GROUP, SEG),...]
where the time goes in v2:
time: 68.9 us; the launch traced here: 68.7 us
  Pallas kernels  68.1 us (99%)
    pallas_call x1, Pallas kernels, local(): pl.pallas_call(layer, out_shape=(rows, jax.ShapeDtypeStruct((GROUP, SEG),...  66 us
    pallas_call x1, Pallas kernels, local(): pl.pallas_call(functools.partial(finish, factor), out_shape=(rows, jax.Sh...  2.13 us

profile of v2, /device:TPU:1, one launch (start us, length us, event | category | flops | bytes accessed | tf_op | source)
XLA Modules:
  0.0 68.7 jit_solution(16183048856276707203)
XLA Ops:
  0.6 66.0 %layer.1 = (bf16[24,2048]{1,0:T(8,128)(2,1)}, bf16[192,384]{1,0:T(8,128)(2,1)}, bf16[24,2048]{1,0:T(8,128)(2,1)}, f32[2,264,128]{2,1,0:T(8,128)}) custom-call(bf16[24,2048]{1,0:T(8,128)(2,1)} %xn_in.1, bf16[24,2048]{1,0:T(8,128)(2,1)} %xp_in.1, bf16[24,2048]{1,0:T(8,128)(2,1)} %go_in.1, bf16[64,352]{1,0:T(8,128)(2,1)} %gw_in.1, bf16[64,352]{1,0:T(8,128)(2,1)} %uw_in.1, ...), custom_call_target="tpu_custom_call" | custom-call | tf_op jit(solution)/shard_map/layer/pallas_call | solution.py:686
  66.6 2.1 %finish.1 = (bf16[24,2048]{1,0:T(8,128)(2,1)}, bf16[192,352]{1,0:T(8,128)(2,1)}, bf16[24,2048]{1,0:T(8,128)(2,1)}, f32[64,352]{1,0:T(8,128)}, f32[64,352]{1,0:T(8,128)}, /*index=5*/f32[64,352]{1,0:T(8,128)}) custom-call(bf16[24,2048]{1,0:T(8,128)(2,1)} %get-tuple-element.16.out_in, bf16[192,384]{1,0:T(8,128)(2,1)} %get-tuple-element.17.hid_in, ...), custom_call_target="tpu_custom_call" | custom-call | tf_op jit(solution)/shard_map/finish/pallas_call | solution.py:733

commit v3 on v2

--- a/solution.py
+++ b/solution.py
@@ -30,7 +30,7 @@
 EY = (0, 1, -1, 2)
 REDUCE = (
     (4, 2), (3, 2), (-3, 2), (-2, 2), (2, 2), (4, -1), (4, 1), (-1, 2), (3, -1), (3, 1), (1, 2), (-3, -1), (-3, 1),
-    (0, 2), (-2, -1), (-2, 1), (2, -1), (2, 1), (4, 0), (-1, -1), (-1, 1), (3, 0), (-3, 0), (1, -1), (1, 1), (0, -1),
+    (4, 0), (0, 2), (-2, -1), (-2, 1), (3, 0), (2, -1), (2, 1), (-1, -1), (-1, 1), (-3, 0), (1, -1), (1, 1), (0, -1),
     (0, 1), (-2, 0), (2, 0), (-1, 0), (1, 0),
 )
 
@@ -175,7 +175,7 @@
     for copy in loads:
         copy.start()
 
-    for copy in loads:
+    for copy in loads[0:3]:
         copy.wait()
 
     gate_up_down = [widened(ours[i].astype(F32), SEG) for i in range(3)]
@@ -192,6 +192,9 @@
             own[q, HALF * t:HALF * t + HALF, :] = column.astype(BF16)
         own[q, 256:PACK, :] = folded(last[rows, 384:512]).astype(BF16)
 
+    for copy in loads[3:]:
+        copy.wait()
+
     @pl.when(keeps)
     def _():
         w[me] = own[...]
@@ -235,18 +238,15 @@
         for a in range(3):
             remote(mine.at[a], tok.at[NB * a + j], hop_s, hop_r.at[a, c], {"c": 1 - c})
 
-    def hop(a):
+    def hop(a, who):
         block = tok.at[NB * a + j]
 
-        @pl.when(moves)
-        def _():
-            remote(mine.at[a], block, hop_s, hop_r.at[a, c], {"z": zp, "c": 1 - c})
-
-        @pl.when(keeps)
-        def _():
-            remote(mine.at[a], block, hop_s, hop_r.at[a, c], {"z": zp})
-
-    hop(0)
+        @pl.when(who)
+        def _():
+            remote(mine.at[a], block, hop_s, hop_r.at[a, c], {"z": zp, "c": par})
+
+    hop(0, c >= 0)
+    hop(1, moves)
 
     @pl.when(moves)
     def _():
@@ -261,7 +261,7 @@
                 def _():
                     own_sends(2)
 
-                hop(1)
+                hop(1, keeps)
 
             lo, hi = rows_of(m)
             piece = w.at[ch, c, pl.ds(lo, hi - lo)]
@@ -366,7 +366,7 @@
 
     timed = [
         (1.0, tok_stay, 0), (1.1, tok_stay, 1), (6.4, tok_near, 0, keeps), (6.6, tok_hop, 0), (9.0, tok_near, 1, keeps),
-        (9.1, hop, 2), (10.9, tok_hop, 1), (11.0, tok_near, 0, moves), (15.0, tok_near, 1, moves), (15.1, tok_stay, 2),
+        (9.1, hop, 2, c >= 0), (10.9, tok_hop, 1), (11.0, tok_near, 0, moves), (15.0, tok_near, 1, moves), (15.1, tok_stay, 2),
         (15.2, tok_hop, 2), (16.0, tok_last, 0), (19.7, tok_last, 1), (22.5, tok_near, 2, c >= 0),
     ]
     for i, (n, t) in enumerate(order):
@@ -569,8 +569,8 @@
     plan += [(9, share_next, 0), (9, share_on, 1, 0), (10, share_next, 1), (10, share_next, 2), (11, share_next, 3)]
     plan += [(11, share_next, 4), (12, share_next, 5), (12, share_on, 1, 1), (13, share_next, 6), (13, share_next, 7)]
     plan += [
-        (19, share_plane, 1, 0), (22, share_on, 0, 0), (23, share_plane, 1, 1), (26, share_on, 0, 1),
-        (27, hidden_out), (28, share_plane, 0, 0), (29, share_plane, 0, 1),
+        (20, share_plane, 1, 0), (22, share_on, 0, 0), (25, share_plane, 1, 1), (29, share_on, 0, 1),
+        (29, hidden_out), (29, share_plane, 0, 0), (31, share_plane, 0, 1),
         (92, share_final, 1, gin_ref), (93, share_final, 0, out_ref),
     ]
 

time: 68.9 us -> 67.4 us (0.978)
  Pallas kernels: 68.1 us -> 66.6 us
    pallas_call x1, Pallas kernels: 66 us -> 64.5 us  [local(): pl.pallas_call(layer, out_shape=(rows, jax.ShapeDtypeStruct((GROUP, SEG),...]
where the time goes in v3:
time: 67.4 us; the launch traced here: 67.2 us
  Pallas kernels  66.6 us (99%)
    pallas_call x1, Pallas kernels, local(): pl.pallas_call(layer, out_shape=(rows, jax.ShapeDtypeStruct((GROUP, SEG),...  64.5 us
    pallas_call x1, Pallas kernels, local(): pl.pallas_call(functools.partial(finish, factor), out_shape=(rows, jax.Sh...  2.13 us

profile of v3, /device:TPU:1, one launch (start us, length us, event | category | flops | bytes accessed | tf_op | source)
XLA Modules:
  0.0 67.2 jit_solution(3374239496712241174)
XLA Ops:
  0.6 64.5 %layer.1 = (bf16[24,2048]{1,0:T(8,128)(2,1)}, bf16[192,384]{1,0:T(8,128)(2,1)}, bf16[24,2048]{1,0:T(8,128)(2,1)}, f32[2,264,128]{2,1,0:T(8,128)}) custom-call(bf16[24,2048]{1,0:T(8,128)(2,1)} %xn_in.1, bf16[24,2048]{1,0:T(8,128)(2,1)} %xp_in.1, bf16[24,2048]{1,0:T(8,128)(2,1)} %go_in.1, bf16[64,352]{1,0:T(8,128)(2,1)} %gw_in.1, bf16[64,352]{1,0:T(8,128)(2,1)} %uw_in.1, ...), custom_call_target="tpu_custom_call" | custom-call | tf_op jit(solution)/shard_map/layer/pallas_call | solution.py:686
  65.1 2.1 %finish.1 = (bf16[24,2048]{1,0:T(8,128)(2,1)}, bf16[192,352]{1,0:T(8,128)(2,1)}, bf16[24,2048]{1,0:T(8,128)(2,1)}, f32[64,352]{1,0:T(8,128)}, f32[64,352]{1,0:T(8,128)}, /*index=5*/f32[64,352]{1,0:T(8,128)}) custom-call(bf16[24,2048]{1,0:T(8,128)(2,1)} %get-tuple-element.16.out_in, bf16[192,384]{1,0:T(8,128)(2,1)} %get-tuple-element.17.hid_in, ...), custom_call_target="tpu_custom_call" | custom-call | tf_op jit(solution)/shard_map/finish/pallas_call | solution.py:733

commit v4 on v3

--- a/solution.py
+++ b/solution.py
@@ -366,7 +366,7 @@
 
     timed = [
         (1.0, tok_stay, 0), (1.1, tok_stay, 1), (6.4, tok_near, 0, keeps), (6.6, tok_hop, 0), (9.0, tok_near, 1, keeps),
-        (9.1, hop, 2, c >= 0), (10.9, tok_hop, 1), (11.0, tok_near, 0, moves), (15.0, tok_near, 1, moves), (15.1, tok_stay, 2),
+        (10.9, tok_hop, 1), (11.0, tok_near, 0, moves), (12.3, hop, 2, c >= 0), (15.0, tok_near, 1, moves), (15.1, tok_stay, 2),
         (15.2, tok_hop, 2), (16.0, tok_last, 0), (19.7, tok_last, 1), (22.5, tok_near, 2, c >= 0),
     ]
     for i, (n, t) in enumerate(order):
@@ -627,7 +627,7 @@
             home[q] = (
                 home[q] + far_sum[0, q].astype(F32) + far_sum[1, q].astype(F32)
             )
-        put(home, wg_out, 3)
+            put(home.at[q], wg_out.at[q], 3 + q)
     with jax.named_scope("drain"):
         routed = sum(rows_of(m)[1] - rows_of(m)[0] for m in ids if m[1] or abs(m[0]) > 2) // PACK
         for count, sem in ((routed, ag_s), (routed, rs_s), (4, top_s), (4, back_s), (NZ * NY - 1, twin_s)):
@@ -649,7 +649,7 @@
             expect(tok.at[pl.ds(0, 4)], plane_s)
             expect(hid, hid_s)
 
-        for i, (src, dst) in enumerate(((outv.at[0], out_ref), (outv.at[1], gin_ref), (hid, hid_ref), (home, wg_out))):
+        for i, (src, dst) in enumerate(((outv.at[0], out_ref), (outv.at[1], gin_ref), (hid, hid_ref), *((home.at[q], wg_out.at[q]) for q in range(NC)))):
             pltpu.make_async_copy(src, dst, out_s.at[i]).wait()
 
 
@@ -722,7 +722,7 @@
             dma, dma((len(ids),)), dma, dma, dma, dma((len(EZ),)), dma, dma((3, NC)), dma, dma((3, 4)),
             dma, dma((len(EZ),)), dma, dma((len(ids),)), dma, dma((2, NC)), dma, dma,
             dma, dma((2, 2, 6)), dma, dma((2, 2, 2)),
-            dma, dma, dma((4,)), dma((6,)),
+            dma, dma, dma((5,)), dma((6,)),
         ],
         compiler_params=pltpu.CompilerParams(
             collective_id=0, has_side_effects=True, vmem_limit_bytes=60 * 1024 * 1024

time: 67.4 us -> 67.4 us (level)
  no operation moved by 1% of the time
where the time goes in v4:
time: 67.4 us; the launch traced here: 67.2 us
  Pallas kernels  66.6 us (99%)
    pallas_call x1, Pallas kernels, local(): pl.pallas_call(layer, out_shape=(rows, jax.ShapeDtypeStruct((GROUP, SEG),...  64.5 us
    pallas_call x1, Pallas kernels, local(): pl.pallas_call(functools.partial(finish, factor), out_shape=(rows, jax.Sh...  2.13 us

profile of v4, /device:TPU:1, one launch (start us, length us, event | category | flops | bytes accessed | tf_op | source)
XLA Modules:
  0.0 67.2 jit_solution(6527350959075562944)
XLA Ops:
  0.6 64.5 %layer.1 = (bf16[24,2048]{1,0:T(8,128)(2,1)}, bf16[192,384]{1,0:T(8,128)(2,1)}, bf16[24,2048]{1,0:T(8,128)(2,1)}, f32[2,264,128]{2,1,0:T(8,128)}) custom-call(bf16[24,2048]{1,0:T(8,128)(2,1)} %xn_in.1, bf16[24,2048]{1,0:T(8,128)(2,1)} %xp_in.1, bf16[24,2048]{1,0:T(8,128)(2,1)} %go_in.1, bf16[64,352]{1,0:T(8,128)(2,1)} %gw_in.1, bf16[64,352]{1,0:T(8,128)(2,1)} %uw_in.1, ...), custom_call_target="tpu_custom_call" | custom-call | tf_op jit(solution)/shard_map/layer/pallas_call | solution.py:686
  65.1 2.1 %finish.1 = (bf16[24,2048]{1,0:T(8,128)(2,1)}, bf16[192,352]{1,0:T(8,128)(2,1)}, bf16[24,2048]{1,0:T(8,128)(2,1)}, f32[64,352]{1,0:T(8,128)}, f32[64,352]{1,0:T(8,128)}, /*index=5*/f32[64,352]{1,0:T(8,128)}) custom-call(bf16[24,2048]{1,0:T(8,128)(2,1)} %get-tuple-element.16.out_in, bf16[192,384]{1,0:T(8,128)(2,1)} %get-tuple-element.17.hid_in, ...), custom_call_target="tpu_custom_call" | custom-call | tf_op jit(solution)/shard_map/finish/pallas_call | solution.py:733
